TPU v7x, 32 devices: a whole 2x2x4 slice. The times are simulated.
32 devices in a mesh: sp: 8 (over z, x), tp: 4 (over y, core).
Axes of the slice: x: 2, y: 2, z: 4, core: 2. Of those that a mesh axis runs over, the one named last changes fastest.
Arguments:
- stream: bfloat16 [1024, 2048], P('sp', 'tp')
- norm_gain: float32 [2048], P('tp'), may hold values from 0.1 to 1.9
- w_value: bfloat16 [2048, 512], P(None, 'tp'), may hold values from -0.125 to 0.125
- w_mix: bfloat16 [2048, 512], P(None, 'tp'), may hold values from -0.125 to 0.125
- w_gate: bfloat16 [2048, 512], P(None, 'tp'), may hold values from -0.125 to 0.125
- w_state: bfloat16 [2048, 512], P(None, 'tp'), may hold values from -0.125 to 0.125
- conv_taps: float32 [3, 512], P(None, 'tp'), may hold values from -3 to 3
- skip_gain: float32 [512], P('tp'), may hold values from -3 to 3
- decay_rate: float32 [2, 32, 64], P(None, 'tp'), as said below
- turn_rate: float32 [2, 32, 64], P(None, 'tp'), may hold values from 0.25 to 1.5
- input_real: float32 [2, 32, 64, 16], P(None, 'tp')
- input_imag: float32 [2, 32, 64, 16], P(None, 'tp')
- read_real: float32 [2, 32, 16, 64], P(None, 'tp'), may hold values from -0.75 to 0.75
- read_imag: float32 [2, 32, 16, 64], P(None, 'tp'), may hold values from -0.75 to 0.75
- initial_state: float32 [2, 2, 32, 64], P(None, None, 'tp'), may hold values from -5 to 5
- intervals: float32 [1024], P('sp'), as said below
- proj_conv: bfloat16 [512, 2048], P('tp'), may hold values from -0.1875 to 0.1875
- proj_state: bfloat16 [512, 2048], P('tp'), may hold values from -0.1875 to 0.1875
Outputs:
- mixed: bfloat16 [1024, 2048], P('sp', 'tp')
Inputs may be any that keep to these rules, and one draw needn't show every extreme that they name: `decay_rate`: Positive. `intervals`: Positive.
All inputs are finite; a program needn't handle non-finite values.
Results may differ from a plain program's by a relative error of at most 0.024.
Values may be sent and summed in bfloat16 or wider, within the bound.
A program may use at most 64 MiB of HBM per device.

v0:
```python
import jax
import jax.numpy as jnp
from jax import lax
from jax.sharding import PartitionSpec as P

D = 2048


EPSILON = 1e-06
HIGH = lax.Precision.HIGHEST


def padded_2(shard, sides, width):
    for axis, dim in sides:
        size, length = (lax.axis_size(axis), shard.shape[dim])
        up = [(i, (i + 1) % size) for i in range(size - 1)]
        down = [(j, i) for i, j in up]
        last = lax.slice_in_dim(shard, length - width, length, axis=dim)
        first = lax.slice_in_dim(shard, 0, width, axis=dim)
        before = lax.ppermute(last, axis, up)
        after = lax.ppermute(first, axis, down)
        shard = jnp.concatenate([before, shard, after], axis=dim)
    return shard


def step_factors(decay_rate, turn_rate, interval):
    damping = -decay_rate * interval
    angle = turn_rate * interval
    magnitude = jnp.exp(damping)
    factor_re = magnitude * jnp.cos(angle)
    factor_im = magnitude * jnp.sin(angle)
    half_sine = jnp.sin(0.5 * angle)
    lift_re = jnp.expm1(damping) * jnp.cos(angle) - 2.0 * half_sine * half_sine
    denominator = decay_rate * decay_rate + turn_rate * turn_rate
    gain_real = (turn_rate * factor_im - decay_rate * lift_re) / denominator
    gain_im = -(decay_rate * factor_im + turn_rate * lift_re) / denominator
    return (factor_re, factor_im, gain_real, gain_im)


def advance(elapsed, real_part, imaginary_piece, decay_rate, turn_rate):
    magnitude = jnp.exp(-decay_rate * elapsed)
    angle = turn_rate * elapsed
    cosine = magnitude * jnp.cos(angle)
    sine = magnitude * jnp.sin(angle)
    return (
        cosine * real_part - sine * imaginary_piece,
        sine * real_part + cosine * imaginary_piece,
    )


def chain_rule(decay_rate, turn_rate):

    def compose_edges(earlier, later):
        moved_re, moved_im = advance(later[0], earlier[1], earlier[2], decay_rate, turn_rate)
        return (earlier[0] + later[0], moved_re + later[1], moved_im + later[2])

    return compose_edges


def compose_steps(earlier, later):
    product_re = earlier[0] * later[0] - earlier[1] * later[1]
    product_im = earlier[0] * later[1] + earlier[1] * later[0]
    carried_re = later[0] * earlier[2] - later[1] * earlier[3] + later[2]
    carried_im = later[0] * earlier[3] + later[1] * earlier[2] + later[3]
    return (product_re, product_im, carried_re, carried_im)


def spread_input(matrix, identity_map):
    groups, states, group_width = matrix.shape
    wide = jnp.einsum("gph,gk->ghkp", matrix, identity_map, precision=HIGH)
    return wide.reshape(groups * group_width, groups * states)


def spread_read(matrix, identity_map):
    groups, group_width, states = matrix.shape
    wide = jnp.einsum("ghp,gk->gpkh", matrix, identity_map, precision=HIGH)
    return wide.reshape(groups * states, groups * group_width)


def per_device(
    stream,
    norm_gain,
    w_value,
    w_mix,
    w_gate,
    w_state,
    conv_taps,
    skip_gain,
    decay_rate,
    turn_rate,
    input_real,
    input_imag,
    read_real,
    read_imag,
    initial_state,
    intervals,
    proj_conv,
    proj_state,
):
    row_count = stream.shape[0]
    weights = jnp.concatenate([w_value, w_mix, w_gate, w_state], axis=1)
    widened = stream.astype(jnp.float32)
    squares = lax.psum(jnp.sum(widened * widened, axis=1), "tp")
    inv_rms = lax.rsqrt(squares / D + EPSILON)
    normed = (widened * inv_rms[:, None] * norm_gain).astype(jnp.bfloat16)
    projected = jnp.dot(
        lax.all_gather(normed, "tp", axis=1, tiled=True),
        weights,
        preferred_element_type=jnp.float32,
    )
    channels = w_value.shape[1]
    conv_value = projected[:, :channels].astype(jnp.bfloat16)
    conv_mix = projected[:, channels : 2 * channels].astype(jnp.bfloat16)
    conv_gate = projected[:, 2 * channels : 3 * channels].astype(jnp.bfloat16)
    state_input = projected[:, 3 * channels :].astype(jnp.bfloat16)
    source = (conv_mix.astype(jnp.float32) * conv_value.astype(jnp.float32)).astype(jnp.bfloat16)
    padded = padded_2(source, (("sp", 0),), 1).astype(jnp.float32)
    filtered = conv_taps[0] * padded[:-2] + conv_taps[1] * padded[1:-1] + conv_taps[2] * padded[2:]
    conv_out = (conv_gate.astype(jnp.float32) * filtered).astype(jnp.bfloat16)
    state_float = state_input.astype(jnp.float32)
    identity_map = jnp.eye(decay_rate.shape[1], dtype=jnp.float32)
    position = lax.axis_index("sp")
    final_index = lax.axis_size("sp") - 1
    elapsed = jnp.sum(intervals)
    responses = state_float * skip_gain
    runs = []
    edges = []
    for direction in range(2):
        backward = direction == 1
        rate_vec = decay_rate[direction].reshape(-1)
        turn_vec = turn_rate[direction].reshape(-1)
        factor_re, factor_im, gain_real, gain_im = step_factors(
            rate_vec, turn_vec, intervals[:, None]
        )
        driven_re = jnp.dot(
            state_float, spread_input(input_real[direction], identity_map), precision=HIGH
        )
        driven_im = jnp.dot(
            state_float, spread_input(input_imag[direction], identity_map), precision=HIGH
        )
        push_re = gain_real * driven_re - gain_im * driven_im
        push_im = gain_real * driven_im + gain_im * driven_re
        local_run = lax.associative_scan(
            compose_steps, (factor_re, factor_im, push_re, push_im), reverse=backward, axis=0
        )
        start_re = initial_state[direction, 0].reshape(-1)
        start_im = initial_state[direction, 1].reshape(-1)
        chain_end = position == (final_index if backward else 0)
        entered_re, entered_im = advance(elapsed, start_re, start_im, rate_vec, turn_vec)
        edge_row = 0 if backward else row_count - 1
        edge_re = local_run[2][edge_row] + jnp.where(chain_end, entered_re, 0.0)
        edge_im = local_run[3][edge_row] + jnp.where(chain_end, entered_im, 0.0)
        runs.append((rate_vec, turn_vec, local_run, start_re, start_im, chain_end))
        edges.append((edge_re, edge_im))
    gathered = (
        lax.all_gather(elapsed[None], "sp", axis=0, tiled=True),
        lax.all_gather(edges[0][0][None], "sp", axis=0, tiled=True),
        lax.all_gather(edges[0][1][None], "sp", axis=0, tiled=True),
        lax.all_gather(edges[1][0][None], "sp", axis=0, tiled=True),
        lax.all_gather(edges[1][1][None], "sp", axis=0, tiled=True),
    )
    arrivals = []
    for direction in range(2):
        backward = direction == 1
        prefix = lax.associative_scan(
            chain_rule(runs[direction][0], runs[direction][1]),
            (gathered[0][:, None], gathered[1 + 2 * direction], gathered[2 + 2 * direction]),
            reverse=backward,
            axis=0,
        )
        source_index = position + 1 if backward else position - 1
        valid = (source_index >= 0) & (source_index <= final_index)
        clamped = jnp.clip(source_index, 0, final_index)
        arrive_re = jnp.where(
            valid, lax.dynamic_index_in_dim(prefix[1], clamped, 0, keepdims=False), 0.0
        )
        arrive_im = jnp.where(
            valid, lax.dynamic_index_in_dim(prefix[2], clamped, 0, keepdims=False), 0.0
        )
        arrivals.append((arrive_re, arrive_im))
    for direction in range(2):
        rate_vec, turn_vec, local_run, start_re, start_im, chain_end = runs[direction]
        incoming_re = arrivals[direction][0] + jnp.where(chain_end, start_re, 0.0)
        incoming_im = arrivals[direction][1] + jnp.where(chain_end, start_im, 0.0)
        state_re = local_run[2] + local_run[0] * incoming_re - local_run[1] * incoming_im
        state_im = local_run[3] + local_run[0] * incoming_im + local_run[1] * incoming_re
        responses = responses + jnp.dot(
            state_re, spread_read(read_real[direction], identity_map), precision=HIGH
        )
        responses = responses - jnp.dot(
            state_im, spread_read(read_imag[direction], identity_map), precision=HIGH
        )
    state_out = jax.nn.gelu(responses).astype(jnp.bfloat16)
    branches = jnp.concatenate([conv_out, state_out], axis=1)
    projection = jnp.concatenate([proj_conv, proj_state], axis=0)
    partial_terms = jnp.dot(branches, projection, preferred_element_type=jnp.float32)
    result = lax.psum_scatter(
        partial_terms.astype(jnp.bfloat16), "tp", scatter_dimension=1, tiled=True
    )
    return result


def solution(mesh):
    return jax.shard_map(
        per_device,
        mesh=mesh,
        in_specs=(
            P("sp", "tp"),
            P("tp"),
            P(None, "tp"),
            P(None, "tp"),
            P(None, "tp"),
            P(None, "tp"),
            P(None, "tp"),
            P("tp"),
            P(None, "tp", None),
            P(None, "tp", None),
            P(None, "tp", None, None),
            P(None, "tp", None, None),
            P(None, "tp", None, None),
            P(None, "tp", None, None),
            P(None, None, "tp", None),
            P("sp"),
            P("tp", None),
            P("tp", None),
        ),
        out_specs=P("sp", "tp"),
        check_vma=False,
    )
```

profile of v0, /device:TPU:0, one launch (start us, length us, event | category | flops | bytes accessed | tf_op | source)
XLA Modules:
  0.0 294.0 jit_solution(1675913467936652232)
XLA Ops:
  6.5 1.1 fusion.20
  7.6 8.4 %psum.7 = f32[128]{0:T(128)S(1)} all-reduce(f32[128]{0:T(128)S(1)} %fusion.20), channel_id=1, replica_groups=mesh['sp'=8,'tp'=4] {'tp'}, use_global_device_ids=true, to_apply=%region_1.0 | all-reduce | flops 128 | bytes 1024 | tf_op jit(solution)/shard_map/psum | solution.py:103
  16.1 1.0 fusion.22
  17.1 6.5 %all_gather.18 = bf16[128,2048]{1,0:T(8,128)(2,1)S(1)} all-gather(bf16[128,512]{1,0:T(8,128)(2,1)S(1)} %fusion.22), channel_id=1, replica_groups=mesh['sp'=8,'tp'=4] {'tp'}, dimensions={1}, use_global_device_ids=true | all-gather | bytes 655360 | tf_op jit(solution)/shard_map/all_gather | solution.py:107
  23.6 1.8 fusion.8
  26.7 3.9 %collective-permute-start = (bf16[1,128]{1,0:T(2,128)(2,1)}, bf16[1,128]{1,0:T(2,128)(2,1)}, u32[]{:S(2)}, u32[]{:S(2)}) collective-permute-start(bf16[1,128]{1,0:T(2,128)(2,1)} %get-tuple-element.105), channel_id=1, source_target_pairs={{0,4},{4,8},{8,12},{12,16},{16,20},{20,24},{24,28},{1,5},{5,9},{9,... | collective-permute-start | bytes 776 | tf_op jit(solution)/shard_map/ppermute | solution.py:20
  31.8 1.4 dynamic-update-slice
  33.2 1.3 collective-permute-start.1
  34.4 22.8 %all-reduce.136 = f32[8]{0:T(128)S(1)} all-reduce(f32[8]{0:T(128)S(1)} %dynamic-update-slice), channel_id=1, replica_groups=mesh['sp'=8,'tp'=4] {'sp'}, use_global_device_ids=true, to_apply=%add.136 | all-reduce | flops 8 | bytes 64
  60.4 3.2 %cosine_multiply_fusion.1 = (f32[1,8,64]{2,1,0:T(8,128)}, f32[1,8,64]{2,1,0:T(8,128)}, f32[1,8,64]{2,1,0:T(8,128)}, f32[1,8,64]{2,1,0:T(8,128)}, f32[1,8,64]{2,1...) fusion(f32[]{:T(128)} %bitcast.35, f32[2,8,64]{2,1,0:T(8,128)S(1)} %copy-done.60, ...), kind=kLoop, calls=%fused_computation.390 | loop fusion | flops 8704 | bytes 24592 | tf_op jit(solution)/shard_map/mul | solution.py:43
  64.3 2.6 sine_multiply_fusion
  70.5 5.8 %multiply_add_fusion = (f32[128,512]{1,0:T(8,128)S(1)}, f32[128,512]{1,0:T(8,128)S(1)}, f32[128,512]{1,0:T(8,128)S(1)}, f32[128,512]{1,0:T(8,128)S(1)}, f32[128,...) fusion(f32[128,512]{1,0:T(8,128)S(1)} %copy-done.25, ...), kind=kOutput, calls=%fused_computation.60 | convolution fusion | flops 103809024 | bytes 3195392 | tf_op jit(solution)/shard_map/dot_general | solution.py:135
  78.1 1.3 slice.1376
  97.4 1.3 mul.2117
  98.8 1.3 mul.2120
  100.1 1.3 fusion.124
  102.8 1.3 fusion.106
  104.1 26.2 %all-gather.2 = f32[8,1,512]{2,1,0:T(1,128)S(1)} all-gather(f32[1,1,512]{2,1,0:T(1,128)S(1)} %get-tuple-element.184), channel_id=1, replica_groups=mesh['sp'=8,'tp'=4] {'sp'}, dimensions={0}, use_global_device_ids=true | all-gather | bytes 18432 | tf_op jit(solution)/shard_map/all_gather | solution.py:159
  130.4 26.4 %all-gather.3 = f32[8,1,512]{2,1,0:T(1,128)S(1)} all-gather(f32[1,1,512]{2,1,0:T(1,128)} %get-tuple-element.185), channel_id=1, replica_groups=mesh['sp'=8,'tp'=4] {'sp'}, dimensions={0}, use_global_device_ids=true | all-gather | bytes 18432 | tf_op jit(solution)/shard_map/all_gather | solution.py:160
  162.0 1.2 slice.1493
  184.8 26.1 %all-gather = f32[8,1,512]{2,1,0:T(1,128)S(1)} all-gather(f32[1,1,512]{2,1,0:T(1,128)S(1)} %get-tuple-element.199), channel_id=1, replica_groups=mesh['sp'=8,'tp'=4] {'sp'}, dimensions={0}, use_global_device_ids=true | all-gather | bytes 18432 | tf_op jit(solution)/shard_map/all_gather | solution.py:157
  211.0 26.1 %all-gather.1 = f32[8,1,512]{2,1,0:T(1,128)S(1)} all-gather(f32[1,1,512]{2,1,0:T(1,128)S(1)} %get-tuple-element.200), channel_id=1, replica_groups=mesh['sp'=8,'tp'=4] {'sp'}, dimensions={0}, use_global_device_ids=true | all-gather | bytes 18432 | tf_op jit(solution)/shard_map/all_gather | solution.py:158
  242.8 1.4 rev.33
  247.4 1.4 rev.27
  251.8 1.2 pad.483
  253.0 1.2 pad.486
  254.2 1.2 pad.487
  256.1 1.1 multiply_bitcast_fusion
  257.2 1.9 reshape.555
  262.6 1.1 convolution_add_fusion.1
  267.3 1.1 convolution_convert_fusion
  268.4 18.8 %reduce-scatter.2.cloned.1.call-done = bf16[128,512]{1,0:T(8,128)(2,1)} async-done(((bf16[128,2048]{1,0:T(8,128)(2,1)}), bf16[128,512]{1,0:T(8,128)(2,1)}) %reduce-scatter.2.cloned.1.call-update) | async-done | bytes 131088 | tf_op jit(solution)/shard_map/reduce_scatter | solution.py:197
  (852 shorter events, 73.9 us)
Async XLA Ops:
  6.5 280.6 %reduce-scatter.2.cloned.1.call-start = ((), (), s32[]{:S(2)}) async-start(), calls=%async_computation.1 | async-start | bytes 655360 | tf_op jit(solution)/shard_map/reduce_scatter | solution.py:197
  23.6 36.8 %copy-start.60 = (f32[2,8,64]{2,1,0:T(8,128)S(1)}, f32[2,8,64]{2,1,0:T(8,128)}, u32[]{:S(2)}) copy-start(f32[2,8,64]{2,1,0:T(8,128)} %param.26) | copy-start | bytes 12292
  23.6 36.8 %copy-start.61 = (f32[2,8,64]{2,1,0:T(8,128)S(1)}, f32[2,8,64]{2,1,0:T(8,128)}, u32[]{:S(2)}) copy-start(f32[2,8,64]{2,1,0:T(8,128)} %param.27) | copy-start | bytes 12292
  23.6 43.6 %copy-start.36 = (f32[2,8,64,16]{2,3,1,0:T(8,128)S(1)}, f32[2,8,64,16]{2,3,1,0:T(8,128)}, u32[]{:S(2)}) copy-start(f32[2,8,64,16]{2,3,1,0:T(8,128)} %param.29) | copy-start | bytes 196612
  23.6 43.6 %copy-start.37 = (f32[2,8,64,16]{2,3,1,0:T(8,128)S(1)}, f32[2,8,64,16]{2,3,1,0:T(8,128)}, u32[]{:S(2)}) copy-start(f32[2,8,64,16]{2,3,1,0:T(8,128)} %param.28) | copy-start | bytes 196612
  25.4 44.4 %copy-start.18 = (bf16[128,512]{1,0:T(8,128)(2,1)}, bf16[128,512]{1,0:T(8,128)(2,1)S(1)}, u32[]{:S(2)}) copy-start(bf16[128,512]{1,0:T(8,128)(2,1)S(1)} %fusion.8) | copy-start | bytes 393220
  26.7 239.8 %collective-permute-start = (bf16[1,128]{1,0:T(2,128)(2,1)}, bf16[1,128]{1,0:T(2,128)(2,1)}, u32[]{:S(2)}, u32[]{:S(2)}) collective-permute-start(bf16[1,128]{1,0:T(2,128)(2,1)} %get-tuple-element.105), channel_id=1, source_target_pairs={{0,4},{4,8},{8,12},{12,16},{16,20},{20,24},{24,28},{1,5},{5,9},{9,... | collective-permute-start | bytes 776 | tf_op jit(solution)/shard_map/ppermute | solution.py:20
  33.2 233.3 %collective-permute-start.1 = (bf16[1,128]{1,0:T(2,128)(2,1)}, bf16[1,128]{1,0:T(2,128)(2,1)}, u32[]{:S(2)}, u32[]{:S(2)}) collective-permute-start(bf16[1,128]{1,0:T(2,128)(2,1)} %get-tuple-element.106), channel_id=1, source_target_pairs={{4,0},{8,4},{12,8},{16,12},{20,16},{24,20},{28,24},{5,1},{9,5},{13... | collective-permute-start | bytes 776 | tf_op jit(solution)/shard_map/ppermute | solution.py:21
  104.1 65.9 %copy-start.41 = (f32[3,512]{1,0:T(4,128)S(1)}, f32[3,512]{1,0:T(4,128)}, u32[]{:S(2)}) copy-start(f32[3,512]{1,0:T(4,128)} %copy-done.40) | copy-start | bytes 18436
  104.1 65.9 %copy-start.43 = (f32[3,512]{1,0:T(4,128)S(1)}, f32[3,512]{1,0:T(4,128)}, u32[]{:S(2)}) copy-start(f32[3,512]{1,0:T(4,128)} %copy-done.42) | copy-start | bytes 18436
  104.1 68.2 %copy-start.29 = (f32[7,512]{1,0:T(8,128)S(1)}, f32[7,512]{1,0:T(8,128)}, u32[]{:S(2)}) copy-start(f32[7,512]{1,0:T(8,128)} %copy-done.28) | copy-start | bytes 43012
  183.9 60.3 %copy-start.2 = (f32[128,512]{1,0:T(8,128)}, f32[128,512]{1,0:T(8,128)S(1)}, u32[]{:S(2)}) copy-start(f32[128,512]{1,0:T(8,128)S(1)} %pad.445) | copy-start | bytes 786436
  183.9 53.3 %copy-start.49 = (f32[512]{0:T(512)S(1)}, f32[512]{0:T(512)}, u32[]{:S(2)}) copy-start(f32[512]{0:T(512)} %copy-done.48) | copy-start | bytes 6148
  183.9 53.3 %copy-start.67 = (f32[512]{0:T(512)S(1)}, f32[512]{0:T(512)}, u32[]{:S(2)}) copy-start(f32[512]{0:T(512)} %copy-done.66) | copy-start | bytes 6148
  183.9 53.3 %copy-start.121 = (f32[4,1]{0,1:T(1,128)S(1)}, f32[4,1]{0,1:T(1,128)}, u32[]{:S(2)}) copy-start(f32[4,1]{0,1:T(1,128)} %copy-done.120) | copy-start | bytes 52
  183.9 57.1 %copy-start.132 = (f32[8]{0:T(128)S(1)}, f32[8]{0:T(128)}, u32[]{:S(2)}) copy-start(f32[8]{0:T(128)} %copy-done.131) | copy-start | bytes 100
  184.0 60.9 %copy-start.4 = (f32[128,512]{1,0:T(8,128)}, f32[128,512]{1,0:T(8,128)S(1)}, u32[]{:S(2)}) copy-start(f32[128,512]{1,0:T(8,128)S(1)} %pad.444) | copy-start | bytes 786436
  184.0 60.2 %copy-start.85 = (f32[1,8,64]{2,1,0:T(8,128)S(1)}, f32[1,8,64]{2,1,0:T(8,128)}, u32[]{:S(2)}) copy-start(f32[1,8,64]{2,1,0:T(8,128)} %get-tuple-element.142) | copy-start | bytes 6148
  184.0 60.3 %copy-start.84 = (f32[1,8,64]{2,1,0:T(8,128)S(1)}, f32[1,8,64]{2,1,0:T(8,128)}, u32[]{:S(2)}) copy-start(f32[1,8,64]{2,1,0:T(8,128)} %get-tuple-element.140) | copy-start | bytes 6148
  184.0 60.3 %copy-start.82 = (f32[1,8,64]{2,1,0:T(8,128)S(1)}, f32[1,8,64]{2,1,0:T(8,128)}, u32[]{:S(2)}) copy-start(f32[1,8,64]{2,1,0:T(8,128)} %get-tuple-element.131) | copy-start | bytes 6148
  184.0 60.4 %copy-start.83 = (f32[1,8,64]{2,1,0:T(8,128)S(1)}, f32[1,8,64]{2,1,0:T(8,128)}, u32[]{:S(2)}) copy-start(f32[1,8,64]{2,1,0:T(8,128)} %get-tuple-element.138) | copy-start | bytes 6148
  184.0 60.5 %copy-start.51 = (f32[512]{0:T(512)S(1)}, f32[512]{0:T(512)}, u32[]{:S(2)}) copy-start(f32[512]{0:T(512)} %copy-done.50) | copy-start | bytes 6148
  184.1 60.5 %copy-start.69 = (f32[512]{0:T(512)S(1)}, f32[512]{0:T(512)}, u32[]{:S(2)}) copy-start(f32[512]{0:T(512)} %copy-done.68) | copy-start | bytes 6148
  184.1 60.5 %copy-start.88 = (f32[2,512]{1,0:T(2,128)S(1)}, f32[2,512]{1,0:T(2,128)}, u32[]{:S(2)}) copy-start(f32[2,512]{1,0:T(2,128)} %slice.1509) | copy-start | bytes 12292
  184.1 60.5 %copy-start.89 = (f32[2,512]{1,0:T(2,128)S(1)}, f32[2,512]{1,0:T(2,128)}, u32[]{:S(2)}) copy-start(f32[2,512]{1,0:T(2,128)} %slice.1513) | copy-start | bytes 12292
  184.1 60.5 %copy-start.90 = (f32[2,512]{1,0:T(2,128)S(1)}, f32[2,512]{1,0:T(2,128)}, u32[]{:S(2)}) copy-start(f32[2,512]{1,0:T(2,128)} %slice.1512) | copy-start | bytes 12292
  184.1 60.5 %copy-start.91 = (f32[2,512]{1,0:T(2,128)S(1)}, f32[2,512]{1,0:T(2,128)}, u32[]{:S(2)}) copy-start(f32[2,512]{1,0:T(2,128)} %slice.1517) | copy-start | bytes 12292
  184.1 60.5 %copy-start.119 = (f32[2,1]{0,1:T(1,128)S(1)}, f32[2,1]{0,1:T(1,128)}, u32[]{:S(2)}) copy-start(f32[2,1]{0,1:T(1,128)} %copy-done.118) | copy-start | bytes 28
  184.1 60.7 %copy-start.53 = (f32[4,512]{1,0:T(4,128)S(1)}, f32[4,512]{1,0:T(4,128)}, u32[]{:S(2)}) copy-start(f32[4,512]{1,0:T(4,128)} %copy-done.52) | copy-start | bytes 24580
  184.1 60.7 %copy-start.55 = (f32[4,512]{1,0:T(4,128)S(1)}, f32[4,512]{1,0:T(4,128)}, u32[]{:S(2)}) copy-start(f32[4,512]{1,0:T(4,128)} %copy-done.54) | copy-start | bytes 24580
  184.7 52.4 %copy-start.75 = (f32[1,512]{1,0:T(1,128)}, f32[1,512]{1,0:T(1,128)S(1)}, u32[]{:S(2)}) copy-start(f32[1,512]{1,0:T(1,128)S(1)} %reshape_squeeze.21) | copy-start | bytes 6148
  184.8 52.4 %copy-start.74 = (f32[1,512]{1,0:T(1,128)}, f32[1,512]{1,0:T(1,128)S(1)}, u32[]{:S(2)}) copy-start(f32[1,512]{1,0:T(1,128)S(1)} %reshape_squeeze.22) | copy-start | bytes 6148
  (105 other events, 412.7 us)
Sparse Core Ops, SparseCore 0:
  268.5 18.6 reduce-scatter.1
where the time goes:
time: 296 us; the launch traced here: 294 us
  blocking collectives  143 us (48%)
  local copies, waits for them, and re-layouts  71.1 us (24%)
  other arithmetic  26.4 us (9%)
  waiting for transfers between devices  18.8 us (6%)
  between operations  17.2 us (6%)
  matrix products  12.6 us (4%)
  starting transfers between devices  5.2 us (2%)
    all_gather x1, blocking collectives, per_device(): lax.all_gather(edges[1][1][None], 'sp', axis=0, tiled=True)  26.4 us
    all_gather x1, blocking collectives, per_device(): lax.all_gather(edges[1][0][None], 'sp', axis=0, tiled=True)  26.2 us
    all_gather x1, blocking collectives, per_device(): lax.all_gather(edges[0][0][None], 'sp', axis=0, tiled=True)  26.1 us
    all_gather x1, blocking collectives, per_device(): lax.all_gather(edges[0][1][None], 'sp', axis=0, tiled=True)  26.1 us
    slice x194, local copies, waits for them, and re-layouts, per_device(): lax.associative_scan(compose_steps, (factor_re, factor_im, push_re, push_...  24.4 us
    unnamed x1, blocking collectives  22.8 us
    reduce_scatter x1, waiting for transfers between devices, per_device(): lax.psum_scatter(partial_terms.astype(jnp.bfloat16), 'tp', scatter_dimens...  18.8 us
    slice x44, local copies, waits for them, and re-layouts, per_device(): lax.associative_scan(chain_rule(runs[direction][0], runs[direction][1]),...  15.7 us
  transfers between devices with their start and end apart: 3, of which 1 were waited for; matrix products, arithmetic and copies ran while one was open for 32% of the time, Pallas kernels for 0%

commit v1 on v0

v1 whole, which is shorter than its diff:
```python
import functools

import jax
import jax.numpy as jnp
from jax import lax
from jax.experimental import pallas as pl
from jax.experimental.pallas import tpu as pltpu
from jax.sharding import PartitionSpec as P

EPSILON = 1e-06
MESH = pl.DeviceIdType.MESH
F32 = jnp.float32
BF16 = jnp.bfloat16
CHUNKS = 2
OUT_CHUNKS = 2


def dot(a, b):
    return jnp.dot(a, b, preferred_element_type=F32)


def dot_t(a, b):
    return lax.dot_general(a, b, (((1,), (1,)), ((), ())), preferred_element_type=F32)


def half_turns(angle):
    theta = 0.5 * angle
    n = jnp.floor(theta * 0.6366197723675814 + 0.5)
    r = theta - n * 1.5703125
    r = r - n * 0.00048351287841796875
    r = r - n * 3.1385570764541626e-07
    r = r - n * 6.077100627776710e-11
    odd = (n - 2.0 * jnp.floor(0.5 * n)) > 0.5
    z = r * r
    s = r + r * z * ((-1.9515295891e-4 * z + 8.3321608736e-3) * z - 1.6666654611e-1)
    c = 1.0 - 0.5 * z + z * z * (
        (2.443315711809948e-5 * z - 1.388731625493765e-3) * z + 4.166664568298827e-2
    )
    square = jnp.where(odd, c * c, s * s)
    double = 2.0 * s * c
    return square, jnp.where(odd, -double, double)


def expm1_of(x, e):
    p = 1.0 + x * (1.0 / 7.0)
    for k in (6.0, 5.0, 4.0, 3.0, 2.0):
        p = 1.0 + x * p * (1.0 / k)
    return jnp.where(x > -0.35, x * p, e - 1.0)


def repeat(lo, hi, body):
    if hi - lo <= 16:
        for i in range(lo, hi):
            body(i)
    else:
        def step(i, carry):
            body(i)
            return carry
        lax.fori_loop(lo, hi, step, 0)


def kernel(
    n_sp, n_tp,
    x_ref, gain_ref, wv, wm, wg, ws, taps_ref, skip_ref, decay_ref, turn_ref,
    inr, ini, rdr, rdi, init_ref, iv_s, iv_ref, pc, ps,
    out_ref,
    w_all, p_all, in_v, rd_v, x_full, gains, el_all, fr_ref, fi_ref, gr_ref, gi_ref,
    dr_ref, di_ref, h0r, h0i, h1r, h1i, bt_ref, rt_ref, src_ref, halo_ref, e_out, e_all,
    blk_r, blk_i, p1_out, p1_in, p2_out, p2_in, c_out, c_in,
    load_sem, as_sem, ar_sem, bs_sem, br_sem, fs_sem, fwr_sem, gs_sem, grv_sem,
    is_sem, ir_sem, hs_sem, hr_sem, es_sem, er_sem, p1s, p1r, p2s, p2r, cs, cr,
):
    tp, sp = lax.axis_index("tp"), lax.axis_index("sp")
    rows, width = x_ref.shape
    channels = wv.shape[1]
    y, core = tp // 2, tp % 2
    sib = y * 2 + 1 - core
    oth = (1 - y) * 2 + core
    diag = (1 - y) * 2 + 1 - core
    cw = width // CHUNKS

    loads = []

    def load(src, dst):
        copy = pltpu.make_async_copy(src, dst, load_sem.at[len(loads)])
        copy.start()
        loads.append(copy)

    load(inr, in_v.at[0])
    load(ini, in_v.at[1])
    load(rdr, rd_v.at[0])
    load(rdi, rd_v.at[1])
    for j, w in enumerate((wv, wm, wg, ws)):
        load(w, w_all.at[:, pl.ds(j * channels, channels)])
    load(pc, p_all.at[pl.ds(0, channels)])
    load(ps, p_all.at[pl.ds(channels, channels)])

    barrier = pltpu.get_barrier_semaphore()
    for j in range(1, n_tp):
        pl.semaphore_signal(barrier, inc=1, device_id={"tp": (tp + j) % n_tp}, device_id_type=MESH)
    repeat(1, n_sp, lambda r: pl.semaphore_signal(
        barrier, inc=1, device_id={"sp": (sp + r) % n_sp}, device_id_type=MESH))
    pl.semaphore_wait(barrier, n_tp - 1 + n_sp - 1)

    def remote(src, dst, send, recv, where):
        return pltpu.make_async_remote_copy(
            src_ref=src, dst_ref=dst, send_sem=send, recv_sem=recv,
            device_id=where, device_id_type=MESH)

    to_sib, to_oth, forward = [], [], []
    for c in range(CHUNKS):
        piece = x_ref.at[:, pl.ds(c * cw, cw)]
        to_oth.append(remote(piece, x_full.at[tp, c], bs_sem.at[c], br_sem.at[c], {"tp": oth}))
        to_sib.append(remote(piece, x_full.at[tp, c], as_sem.at[c], ar_sem.at[c], {"tp": sib}))
        forward.append(remote(x_full.at[oth, c], x_full.at[oth, c], fs_sem.at[c], fwr_sem.at[c],
                              {"tp": sib}))
    gain_copies = [
        remote(gain_ref, gains.at[tp], gs_sem.at[j], grv_sem.at[j], {"tp": (tp + j) % n_tp})
        for j in range(1, n_tp)
    ]
    for copy in gain_copies:
        copy.start()
    for c in range(CHUNKS):
        to_oth[c].start()
        to_sib[c].start()

    def interval_copy(r):
        return remote(iv_ref, el_all.at[r], is_sem.at[r], ir_sem.at[r], {"sp": (sp + r) % n_sp})

    repeat(1, n_sp, lambda r: interval_copy(r).start())

    sub = lax.broadcasted_iota(jnp.int32, (8, 128), 0)
    top = sub < 4

    def pack(ref):
        even = ref[pl.ds(0, 8, stride=2), :]
        odd = ref[pl.ds(1, 8, stride=2), :]
        return jnp.concatenate([even, odd], axis=1)

    decay, turn = pack(decay_ref), pack(turn_ref)

    def pack_init(part):
        halves = [
            jnp.concatenate([init_ref[pl.ds(d * 16 + part * 8, 4, stride=2), :],
                             init_ref[pl.ds(d * 16 + part * 8 + 1, 4, stride=2), :]], axis=1)
            for d in range(2)
        ]
        return jnp.concatenate(halves, axis=0)

    init_r, init_i = pack_init(0), pack_init(1)
    den = decay * decay + turn * turn
    td, dd = turn / den, decay / den

    def factors(k, carry):
        iv = jnp.where(top, iv_s[k], iv_s[rows - 1 - k])
        damp = -decay * iv
        square, sine = half_turns(turn * iv)
        e = jnp.exp(damp)
        cosine = 1.0 - 2.0 * square
        f_im = e * sine
        lift = expm1_of(damp, e) * cosine - 2.0 * square
        at = pl.ds(pl.multiple_of(k * 8, 8), 8)
        fr_ref[at, :] = e * cosine
        fi_ref[at, :] = f_im
        gr_ref[at, :] = td * f_im - dd * lift
        gi_ref[at, :] = -(dd * f_im + td * lift)
        return carry

    lax.fori_loop(0, rows, factors, 0, unroll=4)

    for c in range(CHUNKS):
        to_oth[c].wait_recv()
        forward[c].start()

    for i in range(4):
        loads[i].wait()
    states = in_v.shape[1]
    group = in_v.shape[2]
    per = rd_v.shape[2]
    half = states // 2
    spread = (lax.broadcasted_iota(jnp.int32, (group, channels), 1) % group
              == lax.broadcasted_iota(jnp.int32, (group, channels), 0)).astype(BF16)
    keep = ((lax.broadcasted_iota(jnp.int32, (half, channels), 0) // per)
            == (lax.broadcasted_iota(jnp.int32, (half, channels), 1) // group))
    spread_r = (lax.broadcasted_iota(jnp.int32, (per, half), 1) % per
                == lax.broadcasted_iota(jnp.int32, (per, half), 0)).astype(BF16)
    keep_r = ((lax.broadcasted_iota(jnp.int32, (channels, half), 1) // per)
              == (lax.broadcasted_iota(jnp.int32, (channels, half), 0) // group))
    for part in range(2):
        for d in range(2):
            wide = dot(in_v[part, pl.ds(d * half, half), :].astype(BF16), spread)
            bt_ref[part, pl.ds(d * half, half), :] = jnp.where(keep, wide, 0.0).astype(BF16)
            wide = dot(rd_v[part, pl.ds(d * channels, channels), :].astype(BF16), spread_r)
            if part:
                wide = -wide
            rt_ref[part, :, pl.ds(d * half, half)] = jnp.where(keep_r, wide, 0.0).astype(BF16)

    for i in range(4, 8):
        loads[i].wait()
    for copy in gain_copies:
        copy.wait_recv()

    def project(value, gain, first):
        wide = value.astype(F32)
        scaled = (wide * gain).astype(BF16)
        term = dot(scaled, w_all[pl.ds(pl.multiple_of(first, cw), cw), :])
        return term, jnp.sum(wide * wide, axis=1, keepdims=True)

    projected = jnp.zeros((rows, 4 * channels), F32)
    squares = jnp.zeros((rows, 1), F32)
    for c in range(CHUNKS):
        t, s = project(x_ref[:, c * cw:(c + 1) * cw], gain_ref[:, c * cw:(c + 1) * cw],
                       tp * width + c * cw)
        projected, squares = projected + t, squares + s

    def remaining(owner, waits, projected, squares):
        for c in range(CHUNKS):
            if waits is not None:
                waits[c].wait_recv()
            t, s = project(x_full[owner, c], gains[owner][:, c * cw:(c + 1) * cw],
                           owner * width + c * cw)
            projected, squares = projected + t, squares + s
        return projected, squares

    projected, squares = remaining(sib, to_sib, projected, squares)
    projected, squares = remaining(oth, None, projected, squares)
    projected, squares = remaining(diag, forward, projected, squares)
    projected = projected * lax.rsqrt(squares / (width * n_tp) + EPSILON)
    conv_value = projected[:, :channels].astype(BF16).astype(F32)
    conv_mix = projected[:, channels:2 * channels].astype(BF16).astype(F32)
    conv_gate = projected[:, 2 * channels:3 * channels].astype(BF16).astype(F32)
    state_input = projected[:, 3 * channels:].astype(BF16)
    src_ref[...] = (conv_mix * conv_value).astype(BF16)

    for part, ref in ((0, dr_ref), (1, di_ref)):
        driven = dot_t(state_input, bt_ref[part])
        for j in range(8):
            ref[pl.ds(j, rows, stride=8), :] = driven[:, j * 128:(j + 1) * 128]

    halo_up = remote(src_ref.at[pl.ds(rows - 16, 16)], halo_ref.at[0], hs_sem.at[0], hr_sem.at[0],
                     {"sp": (sp + 1) % n_sp})
    halo_down = remote(src_ref.at[pl.ds(0, 16)], halo_ref.at[1], hs_sem.at[1], hr_sem.at[1],
                       {"sp": (sp + n_sp - 1) % n_sp})
    halo_up.start()
    halo_down.start()

    def first_pass(k, carry):
        hr, hi = carry
        at = pl.ds(pl.multiple_of(k * 8, 8), 8)
        back = pl.ds(pl.multiple_of((rows - 1 - k) * 8, 8), 8)
        dr = jnp.where(top, dr_ref[at, :], dr_ref[back, :])
        di = jnp.where(top, di_ref[at, :], di_ref[back, :])
        gr, gi = gr_ref[at, :], gi_ref[at, :]
        fr, fi = fr_ref[at, :], fi_ref[at, :]
        pr = gr * dr - gi * di
        pi = gr * di + gi * dr
        gr_ref[at, :] = pr
        gi_ref[at, :] = pi
        return fr * hr + (pr - fi * hi), fr * hi + (pi + fi * hr)

    zero = jnp.zeros((8, 128), F32)
    hr, hi = lax.fori_loop(0, rows, first_pass, (zero, zero), unroll=8)
    e_out[0] = hr
    e_out[1] = hi

    def edge_copy(r):
        return remote(e_out, e_all.at[r], es_sem.at[r], er_sem.at[r], {"sp": (sp + r) % n_sp})

    repeat(1, n_sp, lambda r: edge_copy(r).start())

    repeat(1, n_sp, lambda r: interval_copy(r).wait_recv())

    def block_factor(r):
        before = jnp.sum(el_all[r], axis=1, keepdims=True) * jnp.where(sp - r >= 0, 1.0, 0.0)
        after = jnp.sum(el_all[n_sp - r], axis=1, keepdims=True) * jnp.where(sp + r < n_sp, 1.0, 0.0)
        elapsed = jnp.where(top, before, after)
        square, sine = half_turns(turn * elapsed)
        e = jnp.exp(-decay * elapsed)
        blk_r[r] = e * (1.0 - 2.0 * square)
        blk_i[r] = e * sine

    repeat(1, n_sp, block_factor)

    halo_up.wait_recv()
    halo_down.wait_recv()
    source = src_ref[...].astype(F32)
    line = lax.broadcasted_iota(jnp.int32, (rows, channels), 0)
    before = halo_ref[0].astype(F32)[15:16, :] * jnp.where(sp > 0, 1.0, 0.0)
    after = halo_ref[1].astype(F32)[0:1, :] * jnp.where(sp < n_sp - 1, 1.0, 0.0)
    previous = jnp.where(line == 0, before, pltpu.roll(source, 1, 0))
    following = jnp.where(line == rows - 1, after, pltpu.roll(source, rows - 1, 0))
    filtered = taps_ref[0:1, :] * previous + taps_ref[1:2, :] * source + taps_ref[2:3, :] * following
    conv_out = (conv_gate * filtered).astype(BF16)
    for i in range(8, 10):
        loads[i].wait()

    repeat(1, n_sp, lambda r: edge_copy(r).wait_recv())

    def combine(r, hr, hi):
        er = jnp.where(top, jnp.where(sp - r >= 0, e_all[r, 0], 0.0),
                       jnp.where(sp + r < n_sp, e_all[n_sp - r, 0], 0.0))
        ei = jnp.where(top, jnp.where(sp - r >= 0, e_all[r, 1], 0.0),
                       jnp.where(sp + r < n_sp, e_all[n_sp - r, 1], 0.0))
        fr, fi = blk_r[r], blk_i[r]
        return fr * hr + (er - fi * hi), fr * hi + (ei + fi * hr)

    hr, hi = init_r, init_i
    if n_sp <= 16:
        for r in range(n_sp - 1, 0, -1):
            hr, hi = combine(r, hr, hi)
    else:
        hr, hi = lax.fori_loop(1, n_sp, lambda i, h: combine(n_sp - i, *h), (hr, hi))

    def second_pass(k, carry):
        hr, hi = carry
        at = pl.ds(pl.multiple_of(k * 8, 8), 8)
        back = pl.ds(pl.multiple_of((rows - 1 - k) * 8, 8), 8)
        fr, fi = fr_ref[at, :], fi_ref[at, :]
        nr = fr * hr + (gr_ref[at, :] - fi * hi)
        ni = fr * hi + (gi_ref[at, :] + fi * hr)
        h0r[at, :] = nr
        h0i[at, :] = ni
        h1r[back, :] = nr
        h1i[back, :] = ni
        return nr, ni

    lax.fori_loop(0, rows, second_pass, (hr, hi), unroll=8)

    response = state_input.astype(F32) * skip_ref[...]
    for part, (forth, back) in enumerate(((h0r, h1r), (h0i, h1i))):
        history = jnp.concatenate(
            [(forth if j < 4 else back)[pl.ds(j, rows, stride=8), :].astype(BF16) for j in range(8)],
            axis=1)
        response = response + dot_t(history, rt_ref[part])
    inner = 0.7978845608028654 * (response + 0.044715 * (response * response * response))
    state_out = (0.5 * response * (1.0 + jnp.tanh(inner))).astype(BF16)
    branches = jnp.concatenate([conv_out, state_out], axis=1)

    ow = width // OUT_CHUNKS

    def partial(owner, c):
        return dot(branches, p_all[:, pl.ds(pl.multiple_of(owner * width + c * ow, ow), ow)])

    first, second, cross = [], [], []
    for c in range(OUT_CHUNKS):
        p1_out[c] = partial(diag, c).astype(BF16)
        first.append(remote(p1_out.at[c], p1_in.at[c], p1s.at[c], p1r.at[c], {"tp": sib}))
        first[c].start()
    kept = [partial(oth, c) for c in range(OUT_CHUNKS)]
    for c in range(OUT_CHUNKS):
        first[c].wait_recv()
        c_out[c] = (kept[c] + p1_in[c].astype(F32)).astype(BF16)
        cross.append(remote(c_out.at[c], c_in.at[c], cs.at[c], cr.at[c], {"tp": oth}))
        cross[c].start()
    for c in range(OUT_CHUNKS):
        p2_out[c] = partial(sib, c).astype(BF16)
        second.append(remote(p2_out.at[c], p2_in.at[c], p2s.at[c], p2r.at[c], {"tp": sib}))
        second[c].start()
    mine = [partial(tp, c) for c in range(OUT_CHUNKS)]
    for c in range(OUT_CHUNKS):
        second[c].wait_recv()
        mine[c] = mine[c] + p2_in[c].astype(F32)
    for c in range(OUT_CHUNKS):
        cross[c].wait_recv()
        out_ref[:, c * ow:(c + 1) * ow] = (mine[c] + c_in[c].astype(F32)).astype(BF16)

    for copy in to_sib + to_oth + forward + gain_copies + [halo_up, halo_down] + first + second + cross:
        copy.wait_send()
    repeat(1, n_sp, lambda r: interval_copy(r).wait_send())
    repeat(1, n_sp, lambda r: edge_copy(r).wait_send())


def per_device(
    n_sp, n_tp,
    stream, norm_gain, w_value, w_mix, w_gate, w_state, conv_taps, skip_gain, decay_rate, turn_rate,
    input_real, input_imag, read_real, read_imag, initial_state, intervals, proj_conv, proj_state,
):
    rows, width = stream.shape
    channels = w_value.shape[1]
    dirs, groups, per, group = input_real.shape
    states = dirs * groups * per
    cw, ow = width // CHUNKS, width // OUT_CHUNKS
    vmem = pl.BlockSpec(memory_space=pltpu.VMEM)
    hbm = pl.BlockSpec(memory_space=pl.ANY)
    smem = pl.BlockSpec(memory_space=pltpu.SMEM)
    dma = lambda n: pltpu.SemaphoreType.DMA((n,))
    packed = pltpu.VMEM((rows * 8, 128), F32)
    return pl.pallas_call(
        functools.partial(kernel, n_sp, n_tp),
        out_shape=jax.ShapeDtypeStruct((rows, width), BF16),
        in_specs=[vmem, vmem, hbm, hbm, hbm, hbm, vmem, vmem, vmem, vmem,
                  hbm, hbm, hbm, hbm, vmem, smem, vmem, hbm, hbm],
        out_specs=vmem,
        scratch_shapes=[
            pltpu.VMEM((width * n_tp, 4 * channels), BF16),
            pltpu.VMEM((2 * channels, width * n_tp), BF16),
            pltpu.VMEM((2, states, group), F32),
            pltpu.VMEM((2, dirs * groups * group, per), F32),
            pltpu.VMEM((n_tp, CHUNKS, rows, cw), BF16),
            pltpu.VMEM((n_tp, 1, width), F32),
            pltpu.VMEM((n_sp, 1, rows), F32),
            packed, packed, packed, packed, packed, packed, packed, packed, packed, packed,
            pltpu.VMEM((2, states, channels), BF16),
            pltpu.VMEM((2, channels, states), BF16),
            pltpu.VMEM((rows, channels), BF16),
            pltpu.VMEM((2, 16, channels), BF16),
            pltpu.VMEM((2, 8, 128), F32),
            pltpu.VMEM((n_sp, 2, 8, 128), F32),
            pltpu.VMEM((n_sp, 8, 128), F32),
            pltpu.VMEM((n_sp, 8, 128), F32),
        ] + [pltpu.VMEM((OUT_CHUNKS, rows, ow), BF16)] * 6 + [
            dma(10),
            dma(CHUNKS), dma(CHUNKS), dma(CHUNKS), dma(CHUNKS), dma(CHUNKS), dma(CHUNKS),
            dma(n_tp), dma(n_tp), dma(n_sp), dma(n_sp), dma(2), dma(2), dma(n_sp), dma(n_sp),
            dma(OUT_CHUNKS), dma(OUT_CHUNKS), dma(OUT_CHUNKS), dma(OUT_CHUNKS),
            dma(OUT_CHUNKS), dma(OUT_CHUNKS),
        ],
        compiler_params=pltpu.CompilerParams(
            collective_id=0, has_side_effects=True, vmem_limit_bytes=48 * 1024 * 1024),
    )(
        stream, norm_gain.reshape(1, width), w_value, w_mix, w_gate, w_state, conv_taps,
        skip_gain.reshape(1, channels),
        decay_rate.reshape(dirs * groups, per), turn_rate.reshape(dirs * groups, per),
        input_real.reshape(states, group), input_imag.reshape(states, group),
        read_real.reshape(dirs * groups * group, per), read_imag.reshape(dirs * groups * group, per),
        initial_state.reshape(dirs * 2 * groups, per), intervals, intervals.reshape(1, rows),
        proj_conv, proj_state,
    )


def solution(mesh):
    return jax.shard_map(
        functools.partial(per_device, mesh.shape["sp"], mesh.shape["tp"]),
        mesh=mesh,
        in_specs=(
            P("sp", "tp"), P("tp"), P(None, "tp"), P(None, "tp"), P(None, "tp"), P(None, "tp"),
            P(None, "tp"), P("tp"), P(None, "tp", None), P(None, "tp", None),
            P(None, "tp", None, None), P(None, "tp", None, None), P(None, "tp", None, None),
            P(None, "tp", None, None), P(None, None, "tp", None), P("sp"), P("tp", None),
            P("tp", None),
        ),
        out_specs=P("sp", "tp"),
        check_vma=False,
    )
```

time: 296 us -> 36.7 us (0.12)
  blocking collectives: 143 us -> 0 us
  local copies, waits for them, and re-layouts: 71.1 us -> 11.5 us
  other arithmetic: 26.4 us -> 0 us
  Pallas kernels: 0 us -> 24.7 us
  waiting for transfers between devices: 18.8 us -> 0 us
  between operations: 17.2 us -> 0.11 us
  matrix products: 12.6 us -> 0 us
  starting transfers between devices: 5.2 us -> 0 us
    all_gather x5 -> x0, blocking collectives: 111 us -> none  [the longest x1 26.4 us: per_device(): lax.all_gather(edges[1][1][None], 'sp', axis=0, tiled=True)]
    slice x240 -> x0, local copies, waits for them, and re-layouts: 42.1 us -> none  [the longest x194 24.4 us: per_device(): lax.associative_scan(compose_steps, (factor_re, factor_im, push_re, push_...]
    pallas_call x0 -> x1, Pallas kernels: none -> 24.7 us  [per_device(): pl.pallas_call(functools.partial(kernel, n_sp, n_tp), out_shape=jax.Shape...]
    unnamed x1 -> x0, blocking collectives: 22.8 us -> none
    reduce_scatter x1 -> x0, waiting for transfers between devices: 18.8 us -> none  [per_device(): lax.psum_scatter(partial_terms.astype(jnp.bfloat16), 'tp', scatter_dimens...]
    dot_general x10 -> x0, matrix products: 12.6 us -> none  [the longest x2 6.13 us: per_device(): jnp.dot(state_float, spread_input(input_real[direction], identity_map), p...]
    add x114 -> x0, other arithmetic: 10.9 us -> none  [the longest x23 2.81 us: compose_steps(): carried_im = later[0] * earlier[3] + later[1] * earlier[2] + later[3]]
    psum x1 -> x0, blocking collectives: 8.4 us -> none  [per_device(): squares = lax.psum(jnp.sum(widened * widened, axis=1), 'tp')]
  transfers between devices with their start and end apart: 3 -> 0, of which waited for: 1 -> 0; matrix products, arithmetic and copies ran while one was open for 32% -> 0% of each run, Pallas kernels for 0% -> 0%
where the time goes in v1:
time: 36.7 us; the launch traced here: 36.2 us
  Pallas kernels  24.7 us (67%)
  local copies, waits for them, and re-layouts  11.5 us (31%)
    pallas_call x1, Pallas kernels, per_device(): pl.pallas_call(functools.partial(kernel, n_sp, n_tp), out_shape=jax.Shape...  24.7 us
    unnamed x35, local copies, waits for them, and re-layouts  11.5 us

profile of v1, /device:TPU:0, one launch (start us, length us, event | category | flops | bytes accessed | tf_op | source)
XLA Modules:
  0.0 36.2 jit_solution(16955551070620419744)
XLA Ops:
  0.0 0.0 copy-start.9
  0.0 0.0 copy-start
  0.0 0.0 copy-start.1
  0.0 1.2 %copy.19 = f32[2,8,64,16]{3,2,1,0:T(8,128)S(1)} copy(f32[2,8,64,16]{2,3,1,0:T(8,128)} %param.28) | data formatting | bytes 131072 | tf_op args[10]
  1.2 0.0 copy-start.6
  1.2 0.0 copy-start.7
  1.2 1.1 %copy.20 = f32[2,8,64,16]{3,2,1,0:T(8,128)S(1)} copy(f32[2,8,64,16]{2,3,1,0:T(8,128)} %param.29) | data formatting | bytes 131072 | tf_op args[11]
  2.4 0.0 copy-start.14
  2.4 0.0 copy-start.15
  2.4 0.0 copy-done.9
  2.4 0.0 copy-done
  2.4 0.0 copy-done.1
  2.4 0.0 copy-done.6
  2.4 0.0 copy-done.7
  2.5 0.6 %copy-done.14 = f32[128]{0:T(128)S(1)} copy-done((f32[128]{0:T(128)S(1)}, f32[128]{0:T(128)}, u32[]{:S(2)}) %copy-start.14) | copy-done | bytes 536
  3.0 0.0 copy-done.15
  3.1 0.0 copy-start.2
  3.1 1.0 %copy-done.2 = bf16[2048,128]{1,0:T(8,128)(2,1)S(1)} copy-done((bf16[2048,128]{1,0:T(8,128)(2,1)S(1)}, bf16[2048,128]{1,0:T(8,128)(2,1)}, u32[]{:S(2)}) %copy-start.2) | copy-done | bytes 524312
  4.1 0.0 copy-start.3
  4.1 1.0 %copy-done.3 = bf16[2048,128]{1,0:T(8,128)(2,1)S(1)} copy-done((bf16[2048,128]{1,0:T(8,128)(2,1)S(1)}, bf16[2048,128]{1,0:T(8,128)(2,1)}, u32[]{:S(2)}) %copy-start.3) | copy-done | bytes 524312
  5.1 0.0 copy-start.4
  5.1 1.0 %copy-done.4 = bf16[128,2048]{1,0:T(8,128)(2,1)S(1)} copy-done((bf16[128,2048]{1,0:T(8,128)(2,1)S(1)}, bf16[128,2048]{1,0:T(8,128)(2,1)}, u32[]{:S(2)}) %copy-start.4) | copy-done | bytes 524312
  6.2 0.0 copy-start.5
  6.2 1.0 %copy-done.5 = bf16[128,2048]{1,0:T(8,128)(2,1)S(1)} copy-done((bf16[128,2048]{1,0:T(8,128)(2,1)S(1)}, bf16[128,2048]{1,0:T(8,128)(2,1)}, u32[]{:S(2)}) %copy-start.5) | copy-done | bytes 524312
  7.2 0.0 copy-start.8
  7.2 0.9 %copy-done.8 = f32[2,8,16,64]{3,2,1,0:T(8,128)S(1)} copy-done((f32[2,8,16,64]{3,2,1,0:T(8,128)S(1)}, f32[2,8,16,64]{3,2,1,0:T(8,128)}, u32[]{:S(2)}) %copy-start.8) | copy-done | bytes 65560
  8.1 0.7 %copy-done.10 = f32[2,8,64]{2,1,0:T(8,128)S(1)} copy-done((f32[2,8,64]{2,1,0:T(8,128)S(1)}, f32[2,8,64]{2,1,0:T(8,128)}, u32[]{:S(2)}) %copy-start.10) | copy-done | bytes 4120
  8.8 0.7 %copy-done.11 = f32[2,8,64]{2,1,0:T(8,128)S(1)} copy-done((f32[2,8,64]{2,1,0:T(8,128)S(1)}, f32[2,8,64]{2,1,0:T(8,128)}, u32[]{:S(2)}) %copy-start.11) | copy-done | bytes 4120
  9.5 0.7 %copy-done.12 = f32[512]{0:T(512)S(1)} copy-done((f32[512]{0:T(512)S(1)}, f32[512]{0:T(512)}, u32[]{:S(2)}) %copy-start.12) | copy-done | bytes 2072
  10.2 0.7 %copy-done.13 = f32[3,128]{1,0:T(4,128)S(1)} copy-done((f32[3,128]{1,0:T(4,128)S(1)}, f32[3,128]{1,0:T(4,128)}, u32[]{:S(2)}) %copy-start.13) | copy-done | bytes 1560
  10.9 24.7 %shard_map.172 = bf16[128,512]{1,0:T(8,128)(2,1)S(1)} custom-call(bf16[128,512]{1,0:T(8,128)(2,1)S(1)} %copy-done.6, f32[1,512]{1,0:T(1,128)S(1)} %bitcast.17, bf16[2048,128]{1,0:T(8,128)(2,1)S(1)} %copy-done, bf16[2048,128]{1,0:T(8,128)(2,1)S(1)} %copy-done.1, bf16[2048,128]{1,0:T(8,128)(2,1)S(1)} %copy-done.2, bf16[2048,128]{1,0:T(8,128)(2,1)S(1)} %copy-done.3, ...), custom_call_target="tpu_custom_call" | custom-call | tf_op jit(solution)/shard_map/pallas_call | solution.py:388
  35.6 0.7 %copy.22 = bf16[128,512]{1,0:T(8,128)(2,1)} copy(bf16[128,512]{1,0:T(8,128)(2,1)S(1)} %shard_map.172) | data formatting | bytes 262144
  (4 shorter events, 0.0 us)
Async XLA Ops:
  0.0 2.4 %copy-start.9 = (f32[2,2,8,64]{3,2,1,0:T(8,128)S(1)}, f32[2,2,8,64]{3,2,1,0:T(8,128)}, u32[]{:S(2)}) copy-start(f32[2,2,8,64]{3,2,1,0:T(8,128)} %param.32) | copy-start | bytes 24580
  0.0 2.4 %copy-start = (bf16[2048,128]{1,0:T(8,128)(2,1)S(1)}, bf16[2048,128]{1,0:T(8,128)(2,1)}, u32[]{:S(2)}) copy-start(bf16[2048,128]{1,0:T(8,128)(2,1)} %wv.1) | copy-start | bytes 1572868
  0.0 2.4 %copy-start.1 = (bf16[2048,128]{1,0:T(8,128)(2,1)S(1)}, bf16[2048,128]{1,0:T(8,128)(2,1)}, u32[]{:S(2)}) copy-start(bf16[2048,128]{1,0:T(8,128)(2,1)} %wm.1) | copy-start | bytes 1572868
  1.2 1.2 %copy-start.6 = (bf16[128,512]{1,0:T(8,128)(2,1)S(1)}, bf16[128,512]{1,0:T(8,128)(2,1)}, u32[]{:S(2)}) copy-start(bf16[128,512]{1,0:T(8,128)(2,1)} %x_ref.1) | copy-start | bytes 393220
  1.2 1.2 %copy-start.7 = (f32[2,8,16,64]{3,2,1,0:T(8,128)S(1)}, f32[2,8,16,64]{3,2,1,0:T(8,128)}, u32[]{:S(2)}) copy-start(f32[2,8,16,64]{3,2,1,0:T(8,128)} %param.30) | copy-start | bytes 196612
  2.4 0.7 %copy-start.14 = (f32[128]{0:T(128)S(1)}, f32[128]{0:T(128)}, u32[]{:S(2)}) copy-start(f32[128]{0:T(128)} %iv_s.1) | copy-start | bytes 1540
  2.4 0.7 %copy-start.15 = (f32[128]{0:T(128)S(1)}, f32[128]{0:T(128)}, u32[]{:S(2)}) copy-start(f32[128]{0:T(128)} %param.25) | copy-start | bytes 1540
  3.1 1.0 %copy-start.2 = (bf16[2048,128]{1,0:T(8,128)(2,1)S(1)}, bf16[2048,128]{1,0:T(8,128)(2,1)}, u32[]{:S(2)}) copy-start(bf16[2048,128]{1,0:T(8,128)(2,1)} %wg.1) | copy-start | bytes 1572868
  4.1 1.0 %copy-start.3 = (bf16[2048,128]{1,0:T(8,128)(2,1)S(1)}, bf16[2048,128]{1,0:T(8,128)(2,1)}, u32[]{:S(2)}) copy-start(bf16[2048,128]{1,0:T(8,128)(2,1)} %ws.1) | copy-start | bytes 1572868
  5.1 1.0 %copy-start.4 = (bf16[128,2048]{1,0:T(8,128)(2,1)S(1)}, bf16[128,2048]{1,0:T(8,128)(2,1)}, u32[]{:S(2)}) copy-start(bf16[128,2048]{1,0:T(8,128)(2,1)} %pc.1) | copy-start | bytes 1572868
  6.2 1.0 %copy-start.5 = (bf16[128,2048]{1,0:T(8,128)(2,1)S(1)}, bf16[128,2048]{1,0:T(8,128)(2,1)}, u32[]{:S(2)}) copy-start(bf16[128,2048]{1,0:T(8,128)(2,1)} %ps.1) | copy-start | bytes 1572868
  7.2 0.9 %copy-start.8 = (f32[2,8,16,64]{3,2,1,0:T(8,128)S(1)}, f32[2,8,16,64]{3,2,1,0:T(8,128)}, u32[]{:S(2)}) copy-start(f32[2,8,16,64]{3,2,1,0:T(8,128)} %param.31) | copy-start | bytes 196612
  8.1 0.7 %copy-start.10 = (f32[2,8,64]{2,1,0:T(8,128)S(1)}, f32[2,8,64]{2,1,0:T(8,128)}, u32[]{:S(2)}) copy-start(f32[2,8,64]{2,1,0:T(8,128)} %param.26) | copy-start | bytes 12292
  8.8 0.7 %copy-start.11 = (f32[2,8,64]{2,1,0:T(8,128)S(1)}, f32[2,8,64]{2,1,0:T(8,128)}, u32[]{:S(2)}) copy-start(f32[2,8,64]{2,1,0:T(8,128)} %param.27) | copy-start | bytes 12292
  9.5 0.7 %copy-start.12 = (f32[512]{0:T(512)S(1)}, f32[512]{0:T(512)}, u32[]{:S(2)}) copy-start(f32[512]{0:T(512)} %param.19) | copy-start | bytes 6148
  10.2 0.7 %copy-start.13 = (f32[3,128]{1,0:T(4,128)S(1)}, f32[3,128]{1,0:T(4,128)}, u32[]{:S(2)}) copy-start(f32[3,128]{1,0:T(4,128)} %taps_ref.1) | copy-start | bytes 4612

commit v2 on v1

--- a/solution.py
+++ b/solution.py
@@ -61,9 +61,10 @@
 
 def kernel(
     n_sp, n_tp,
-    x_ref, gain_ref, wv, wm, wg, ws, taps_ref, skip_ref, decay_ref, turn_ref,
-    inr, ini, rdr, rdi, init_ref, iv_s, iv_ref, pc, ps,
+    x_hbm, gain_hbm, wv, wm, wg, ws, taps_hbm, skip_hbm, decay_hbm, turn_hbm,
+    inr, ini, rdr, rdi, init_hbm, iv_hbm, pc, ps,
     out_ref,
+    x_ref, gain_ref, taps_ref, skip_ref, decay_ref, turn_ref, init_ref, iv_s,
     w_all, p_all, in_v, rd_v, x_full, gains, el_all, fr_ref, fi_ref, gr_ref, gi_ref,
     dr_ref, di_ref, h0r, h0i, h1r, h1i, bt_ref, rt_ref, src_ref, halo_ref, e_out, e_all,
     blk_r, blk_i, p1_out, p1_in, p2_out, p2_in, c_out, c_in,
@@ -71,7 +72,7 @@
     is_sem, ir_sem, hs_sem, hr_sem, es_sem, er_sem, p1s, p1r, p2s, p2r, cs, cr,
 ):
     tp, sp = lax.axis_index("tp"), lax.axis_index("sp")
-    rows, width = x_ref.shape
+    rows, width = x_hbm.shape
     channels = wv.shape[1]
     y, core = tp // 2, tp % 2
     sib = y * 2 + 1 - core
@@ -86,20 +87,27 @@
         copy.start()
         loads.append(copy)
 
-    load(inr, in_v.at[0])
-    load(ini, in_v.at[1])
-    load(rdr, rd_v.at[0])
-    load(rdi, rd_v.at[1])
-    for j, w in enumerate((wv, wm, wg, ws)):
-        load(w, w_all.at[:, pl.ds(j * channels, channels)])
-    load(pc, p_all.at[pl.ds(0, channels)])
-    load(ps, p_all.at[pl.ds(channels, channels)])
-
     barrier = pltpu.get_barrier_semaphore()
     for j in range(1, n_tp):
         pl.semaphore_signal(barrier, inc=1, device_id={"tp": (tp + j) % n_tp}, device_id_type=MESH)
     repeat(1, n_sp, lambda r: pl.semaphore_signal(
         barrier, inc=1, device_id={"sp": (sp + r) % n_sp}, device_id_type=MESH))
+    load(iv_hbm, iv_s)
+    load(decay_hbm, decay_ref)
+    load(turn_hbm, turn_ref)
+    load(init_hbm, init_ref)
+    load(inr, in_v.at[0])
+    load(ini, in_v.at[1])
+    load(rdr, rd_v.at[0])
+    load(rdi, rd_v.at[1])
+    load(x_hbm, x_ref)
+    load(gain_hbm, gain_ref)
+    for j, w in enumerate((wv, wm, wg, ws)):
+        load(w, w_all.at[:, pl.ds(j * channels, channels)])
+    load(taps_hbm, taps_ref)
+    load(skip_hbm, skip_ref)
+    load(pc, p_all.at[pl.ds(0, channels)])
+    load(ps, p_all.at[pl.ds(channels, channels)])
     pl.semaphore_wait(barrier, n_tp - 1 + n_sp - 1)
 
     def remote(src, dst, send, recv, where):
@@ -109,13 +117,13 @@
 
     to_sib, to_oth, forward = [], [], []
     for c in range(CHUNKS):
-        piece = x_ref.at[:, pl.ds(c * cw, cw)]
+        piece = x_hbm.at[:, pl.ds(c * cw, cw)]
         to_oth.append(remote(piece, x_full.at[tp, c], bs_sem.at[c], br_sem.at[c], {"tp": oth}))
         to_sib.append(remote(piece, x_full.at[tp, c], as_sem.at[c], ar_sem.at[c], {"tp": sib}))
         forward.append(remote(x_full.at[oth, c], x_full.at[oth, c], fs_sem.at[c], fwr_sem.at[c],
                               {"tp": sib}))
     gain_copies = [
-        remote(gain_ref, gains.at[tp], gs_sem.at[j], grv_sem.at[j], {"tp": (tp + j) % n_tp})
+        remote(gain_hbm, gains.at[tp], gs_sem.at[j], grv_sem.at[j], {"tp": (tp + j) % n_tp})
         for j in range(1, n_tp)
     ]
     for copy in gain_copies:
@@ -125,7 +133,7 @@
         to_sib[c].start()
 
     def interval_copy(r):
-        return remote(iv_ref, el_all.at[r], is_sem.at[r], ir_sem.at[r], {"sp": (sp + r) % n_sp})
+        return remote(iv_hbm, el_all.at[r], is_sem.at[r], ir_sem.at[r], {"sp": (sp + r) % n_sp})
 
     repeat(1, n_sp, lambda r: interval_copy(r).start())
 
@@ -137,6 +145,8 @@
         odd = ref[pl.ds(1, 8, stride=2), :]
         return jnp.concatenate([even, odd], axis=1)
 
+    for i in range(4):
+        loads[i].wait()
     decay, turn = pack(decay_ref), pack(turn_ref)
 
     def pack_init(part):
@@ -152,7 +162,7 @@
     td, dd = turn / den, decay / den
 
     def factors(k, carry):
-        iv = jnp.where(top, iv_s[k], iv_s[rows - 1 - k])
+        iv = jnp.where(top, iv_s[0, k], iv_s[0, rows - 1 - k])
         damp = -decay * iv
         square, sine = half_turns(turn * iv)
         e = jnp.exp(damp)
@@ -166,36 +176,32 @@
         gi_ref[at, :] = -(dd * f_im + td * lift)
         return carry
 
-    lax.fori_loop(0, rows, factors, 0, unroll=4)
-
     for c in range(CHUNKS):
+        lax.fori_loop(c * rows // CHUNKS, (c + 1) * rows // CHUNKS, factors, 0, unroll=4)
         to_oth[c].wait_recv()
         forward[c].start()
 
-    for i in range(4):
+    for i in range(4, 8):
         loads[i].wait()
-    states = in_v.shape[1]
-    group = in_v.shape[2]
+    states = bt_ref.shape[2]
     per = rd_v.shape[2]
     half = states // 2
-    spread = (lax.broadcasted_iota(jnp.int32, (group, channels), 1) % group
-              == lax.broadcasted_iota(jnp.int32, (group, channels), 0)).astype(BF16)
-    keep = ((lax.broadcasted_iota(jnp.int32, (half, channels), 0) // per)
-            == (lax.broadcasted_iota(jnp.int32, (half, channels), 1) // group))
-    spread_r = (lax.broadcasted_iota(jnp.int32, (per, half), 1) % per
-                == lax.broadcasted_iota(jnp.int32, (per, half), 0)).astype(BF16)
-    keep_r = ((lax.broadcasted_iota(jnp.int32, (channels, half), 1) // per)
-              == (lax.broadcasted_iota(jnp.int32, (channels, half), 0) // group))
+    group = channels * per // half
+    spread = (lax.broadcasted_iota(jnp.int32, (per, half), 1) % per
+              == lax.broadcasted_iota(jnp.int32, (per, half), 0)).astype(BF16)
+    keep = ((lax.broadcasted_iota(jnp.int32, (channels, half), 1) // per)
+            == (lax.broadcasted_iota(jnp.int32, (channels, half), 0) // group))
     for part in range(2):
         for d in range(2):
-            wide = dot(in_v[part, pl.ds(d * half, half), :].astype(BF16), spread)
-            bt_ref[part, pl.ds(d * half, half), :] = jnp.where(keep, wide, 0.0).astype(BF16)
-            wide = dot(rd_v[part, pl.ds(d * channels, channels), :].astype(BF16), spread_r)
+            at, to = pl.ds(d * channels, channels), pl.ds(d * half, half)
+            wide = dot(in_v[part, at, :].astype(BF16), spread)
+            bt_ref[part, :, to] = jnp.where(keep, wide, 0.0).astype(BF16)
+            wide = dot(rd_v[part, at, :].astype(BF16), spread)
             if part:
                 wide = -wide
-            rt_ref[part, :, pl.ds(d * half, half)] = jnp.where(keep_r, wide, 0.0).astype(BF16)
-
-    for i in range(4, 8):
+            rt_ref[part, :, to] = jnp.where(keep, wide, 0.0).astype(BF16)
+
+    for i in range(8, 14):
         loads[i].wait()
     for copy in gain_copies:
         copy.wait_recv()
@@ -233,7 +239,7 @@
     src_ref[...] = (conv_mix * conv_value).astype(BF16)
 
     for part, ref in ((0, dr_ref), (1, di_ref)):
-        driven = dot_t(state_input, bt_ref[part])
+        driven = dot(state_input, bt_ref[part])
         for j in range(8):
             ref[pl.ds(j, rows, stride=8), :] = driven[:, j * 128:(j + 1) * 128]
 
@@ -283,6 +289,8 @@
 
     halo_up.wait_recv()
     halo_down.wait_recv()
+    for i in range(14, 18):
+        loads[i].wait()
     source = src_ref[...].astype(F32)
     line = lax.broadcasted_iota(jnp.int32, (rows, channels), 0)
     before = halo_ref[0].astype(F32)[15:16, :] * jnp.where(sp > 0, 1.0, 0.0)
@@ -291,8 +299,6 @@
     following = jnp.where(line == rows - 1, after, pltpu.roll(source, rows - 1, 0))
     filtered = taps_ref[0:1, :] * previous + taps_ref[1:2, :] * source + taps_ref[2:3, :] * following
     conv_out = (conv_gate * filtered).astype(BF16)
-    for i in range(8, 10):
-        loads[i].wait()
 
     repeat(1, n_sp, lambda r: edge_copy(r).wait_recv())
 
@@ -380,27 +386,33 @@
     dirs, groups, per, group = input_real.shape
     states = dirs * groups * per
     cw, ow = width // CHUNKS, width // OUT_CHUNKS
-    vmem = pl.BlockSpec(memory_space=pltpu.VMEM)
-    hbm = pl.BlockSpec(memory_space=pl.ANY)
-    smem = pl.BlockSpec(memory_space=pltpu.SMEM)
+    hbm = pl.BlockSpec(memory_space=pltpu.HBM)
     dma = lambda n: pltpu.SemaphoreType.DMA((n,))
     packed = pltpu.VMEM((rows * 8, 128), F32)
+    rows_of = lambda m: jnp.swapaxes(m, 2, 3).reshape(dirs * groups * group, per)
     return pl.pallas_call(
         functools.partial(kernel, n_sp, n_tp),
         out_shape=jax.ShapeDtypeStruct((rows, width), BF16),
-        in_specs=[vmem, vmem, hbm, hbm, hbm, hbm, vmem, vmem, vmem, vmem,
-                  hbm, hbm, hbm, hbm, vmem, smem, vmem, hbm, hbm],
-        out_specs=vmem,
+        in_specs=[hbm] * 18,
+        out_specs=pl.BlockSpec(memory_space=pltpu.VMEM),
         scratch_shapes=[
+            pltpu.VMEM((rows, width), BF16),
+            pltpu.VMEM((1, width), F32),
+            pltpu.VMEM(conv_taps.shape, F32),
+            pltpu.VMEM((1, channels), F32),
+            pltpu.VMEM((dirs * groups, per), F32),
+            pltpu.VMEM((dirs * groups, per), F32),
+            pltpu.VMEM((dirs * 2 * groups, per), F32),
+            pltpu.SMEM((1, rows), F32),
             pltpu.VMEM((width * n_tp, 4 * channels), BF16),
             pltpu.VMEM((2 * channels, width * n_tp), BF16),
-            pltpu.VMEM((2, states, group), F32),
+            pltpu.VMEM((2, dirs * groups * group, per), F32),
             pltpu.VMEM((2, dirs * groups * group, per), F32),
             pltpu.VMEM((n_tp, CHUNKS, rows, cw), BF16),
             pltpu.VMEM((n_tp, 1, width), F32),
             pltpu.VMEM((n_sp, 1, rows), F32),
             packed, packed, packed, packed, packed, packed, packed, packed, packed, packed,
-            pltpu.VMEM((2, states, channels), BF16),
+            pltpu.VMEM((2, channels, states), BF16),
             pltpu.VMEM((2, channels, states), BF16),
             pltpu.VMEM((rows, channels), BF16),
             pltpu.VMEM((2, 16, channels), BF16),
@@ -409,21 +421,21 @@
             pltpu.VMEM((n_sp, 8, 128), F32),
             pltpu.VMEM((n_sp, 8, 128), F32),
         ] + [pltpu.VMEM((OUT_CHUNKS, rows, ow), BF16)] * 6 + [
-            dma(10),
+            dma(18),
             dma(CHUNKS), dma(CHUNKS), dma(CHUNKS), dma(CHUNKS), dma(CHUNKS), dma(CHUNKS),
             dma(n_tp), dma(n_tp), dma(n_sp), dma(n_sp), dma(2), dma(2), dma(n_sp), dma(n_sp),
             dma(OUT_CHUNKS), dma(OUT_CHUNKS), dma(OUT_CHUNKS), dma(OUT_CHUNKS),
             dma(OUT_CHUNKS), dma(OUT_CHUNKS),
         ],
         compiler_params=pltpu.CompilerParams(
-            collective_id=0, has_side_effects=True, vmem_limit_bytes=48 * 1024 * 1024),
+            collective_id=0, has_side_effects=True, vmem_limit_bytes=67043328),
     )(
         stream, norm_gain.reshape(1, width), w_value, w_mix, w_gate, w_state, conv_taps,
         skip_gain.reshape(1, channels),
         decay_rate.reshape(dirs * groups, per), turn_rate.reshape(dirs * groups, per),
-        input_real.reshape(states, group), input_imag.reshape(states, group),
+        rows_of(input_real), rows_of(input_imag),
         read_real.reshape(dirs * groups * group, per), read_imag.reshape(dirs * groups * group, per),
-        initial_state.reshape(dirs * 2 * groups, per), intervals, intervals.reshape(1, rows),
+        initial_state.reshape(dirs * 2 * groups, per), intervals.reshape(1, rows),
         proj_conv, proj_state,
     )
 

time: 36.7 us -> 26 us (0.71)
  local copies, waits for them, and re-layouts: 11.5 us -> 1.57 us
  Pallas kernels: 24.7 us -> 24.3 us
    unnamed x35 -> x1, local copies, waits for them, and re-layouts: 11.5 us -> 1.57 us
    pallas_call x1, Pallas kernels: 24.7 us -> 24.3 us  [per_device(): pl.pallas_call(functools.partial(kernel, n_sp, n_tp), out_shape=jax.Shape...]
where the time goes in v2:
time: 26 us; the launch traced here: 25.9 us
  Pallas kernels  24.3 us (93%)
  local copies, waits for them, and re-layouts  1.57 us (6%)
    pallas_call x1, Pallas kernels, per_device(): pl.pallas_call(functools.partial(kernel, n_sp, n_tp), out_shape=jax.Shape...  24.3 us
    unnamed x1, local copies, waits for them, and re-layouts  1.57 us

profile of v2, /device:TPU:0, one launch (start us, length us, event | category | flops | bytes accessed | tf_op | source)
XLA Modules:
  0.0 25.9 jit_solution(17166150969556777989)
XLA Ops:
  0.0 24.3 %shard_map.172 = bf16[128,512]{1,0:T(8,128)(2,1)} custom-call(bf16[128,512]{1,0:T(8,128)(2,1)} %x_hbm.1, f32[1,512]{1,0:T(1,128)} %bitcast.21, bf16[2048,128]{1,0:T(8,128)(2,1)} %wv.1, bf16[2048,128]{1,0:T(8,128)(2,1)} %wm.1, bf16[2048,128]{1,0:T(8,128)(2,1)} %wg.1, bf16[2048,128]{1,0:T(8,128)(2,1)} %ws.1, f32[3,128]{1,0:T(4,128)} %taps_hbm.1, ...), custom_call_target="tpu_custom_call" | custom-call | tf_op jit(solution)/shard_map/pallas_call | solution.py:393
  24.3 1.6 %copy.20 = bf16[128,512]{1,0:T(8,128)(2,1)} copy(bf16[128,512]{1,0:T(8,128)(2,1)} %shard_map.172) | data formatting | bytes 262144

commit v3 on v2

--- a/solution.py
+++ b/solution.py
@@ -65,11 +65,11 @@
     inr, ini, rdr, rdi, init_hbm, iv_hbm, pc, ps,
     out_ref,
     x_ref, gain_ref, taps_ref, skip_ref, decay_ref, turn_ref, init_ref, iv_s,
-    w_all, p_all, in_v, rd_v, x_full, gains, el_all, fr_ref, fi_ref, gr_ref, gi_ref,
+    w_all, pc_all, ps_all, so_all, acc_ref, in_v, rd_v, x_full, gains, el_all, fr_ref, fi_ref, gr_ref, gi_ref,
     dr_ref, di_ref, h0r, h0i, h1r, h1i, bt_ref, rt_ref, src_ref, halo_ref, e_out, e_all,
     blk_r, blk_i, p1_out, p1_in, p2_out, p2_in, c_out, c_in,
     load_sem, as_sem, ar_sem, bs_sem, br_sem, fs_sem, fwr_sem, gs_sem, grv_sem,
-    is_sem, ir_sem, hs_sem, hr_sem, es_sem, er_sem, p1s, p1r, p2s, p2r, cs, cr,
+    is_sem, ir_sem, hs_sem, hr_sem, es_sem, er_sem, p1s, p1r, p2s, p2r, cs, cr, ws_sem, wr_sem, os_sem, or_sem,
 ):
     tp, sp = lax.axis_index("tp"), lax.axis_index("sp")
     rows, width = x_hbm.shape
@@ -106,8 +106,8 @@
         load(w, w_all.at[:, pl.ds(j * channels, channels)])
     load(taps_hbm, taps_ref)
     load(skip_hbm, skip_ref)
-    load(pc, p_all.at[pl.ds(0, channels)])
-    load(ps, p_all.at[pl.ds(channels, channels)])
+    load(pc, pc_all)
+    load(ps.at[:, pl.ds(pl.multiple_of(tp * width, width), width)], ps_all.at[tp])
     pl.semaphore_wait(barrier, n_tp - 1 + n_sp - 1)
 
     def remote(src, dst, send, recv, where):
@@ -131,6 +131,16 @@
     for c in range(CHUNKS):
         to_oth[c].start()
         to_sib[c].start()
+
+    weight_copies, state_copies = [], []
+    for j in range(1, n_tp):
+        peer = (tp + j) % n_tp
+        weight_copies.append(remote(
+            ps.at[:, pl.ds(pl.multiple_of(peer * width, width), width)], ps_all.at[tp],
+            ws_sem.at[j], wr_sem.at[j], {"tp": peer}))
+        weight_copies[-1].start()
+        state_copies.append(remote(
+            so_all.at[tp], so_all.at[tp], os_sem.at[j], or_sem.at[j], {"tp": peer}))
 
     def interval_copy(r):
         return remote(iv_hbm, el_all.at[r], is_sem.at[r], ir_sem.at[r], {"sp": (sp + r) % n_sp})
@@ -300,6 +310,29 @@
     filtered = taps_ref[0:1, :] * previous + taps_ref[1:2, :] * source + taps_ref[2:3, :] * following
     conv_out = (conv_gate * filtered).astype(BF16)
 
+    ow = width // OUT_CHUNKS
+
+    def partial(owner, c):
+        return dot(conv_out, pc_all[:, pl.ds(pl.multiple_of(owner * width + c * ow, ow), ow)])
+
+    first, second, cross = [], [], []
+    for c in range(OUT_CHUNKS):
+        p1_out[c] = partial(diag, c).astype(BF16)
+        first.append(remote(p1_out.at[c], p1_in.at[c], p1s.at[c], p1r.at[c], {"tp": sib}))
+        first[c].start()
+    for c in range(OUT_CHUNKS):
+        p2_out[c] = partial(sib, c).astype(BF16)
+        second.append(remote(p2_out.at[c], p2_in.at[c], p2s.at[c], p2r.at[c], {"tp": sib}))
+        second[c].start()
+    for c in range(OUT_CHUNKS):
+        acc_ref[:, c * ow:(c + 1) * ow] = partial(tp, c)
+    kept = [partial(oth, c) for c in range(OUT_CHUNKS)]
+    for c in range(OUT_CHUNKS):
+        first[c].wait_recv()
+        c_out[c] = (kept[c] + p1_in[c].astype(F32)).astype(BF16)
+        cross.append(remote(c_out.at[c], c_in.at[c], cs.at[c], cr.at[c], {"tp": oth}))
+        cross[c].start()
+
     repeat(1, n_sp, lambda r: edge_copy(r).wait_recv())
 
     def combine(r, hr, hi):
@@ -340,37 +373,27 @@
         response = response + dot_t(history, rt_ref[part])
     inner = 0.7978845608028654 * (response + 0.044715 * (response * response * response))
     state_out = (0.5 * response * (1.0 + jnp.tanh(inner))).astype(BF16)
-    branches = jnp.concatenate([conv_out, state_out], axis=1)
-
-    ow = width // OUT_CHUNKS
-
-    def partial(owner, c):
-        return dot(branches, p_all[:, pl.ds(pl.multiple_of(owner * width + c * ow, ow), ow)])
-
-    first, second, cross = [], [], []
-    for c in range(OUT_CHUNKS):
-        p1_out[c] = partial(diag, c).astype(BF16)
-        first.append(remote(p1_out.at[c], p1_in.at[c], p1s.at[c], p1r.at[c], {"tp": sib}))
-        first[c].start()
-    kept = [partial(oth, c) for c in range(OUT_CHUNKS)]
-    for c in range(OUT_CHUNKS):
-        first[c].wait_recv()
-        c_out[c] = (kept[c] + p1_in[c].astype(F32)).astype(BF16)
-        cross.append(remote(c_out.at[c], c_in.at[c], cs.at[c], cr.at[c], {"tp": oth}))
-        cross[c].start()
-    for c in range(OUT_CHUNKS):
-        p2_out[c] = partial(sib, c).astype(BF16)
-        second.append(remote(p2_out.at[c], p2_in.at[c], p2s.at[c], p2r.at[c], {"tp": sib}))
-        second[c].start()
-    mine = [partial(tp, c) for c in range(OUT_CHUNKS)]
+
+    so_all[tp] = state_out
+    for copy in state_copies:
+        copy.start()
+    total = acc_ref[...]
     for c in range(OUT_CHUNKS):
         second[c].wait_recv()
-        mine[c] = mine[c] + p2_in[c].astype(F32)
+    total = total + jnp.concatenate([p2_in[c].astype(F32) for c in range(OUT_CHUNKS)], axis=1)
+    for copy in weight_copies:
+        copy.wait_recv()
+    total = total + dot(state_out, ps_all[tp])
     for c in range(OUT_CHUNKS):
         cross[c].wait_recv()
-        out_ref[:, c * ow:(c + 1) * ow] = (mine[c] + c_in[c].astype(F32)).astype(BF16)
-
-    for copy in to_sib + to_oth + forward + gain_copies + [halo_up, halo_down] + first + second + cross:
+    total = total + jnp.concatenate([c_in[c].astype(F32) for c in range(OUT_CHUNKS)], axis=1)
+    for j in range(1, n_tp):
+        state_copies[j - 1].wait_recv()
+        owner = (tp + n_tp - j) % n_tp
+        total = total + dot(so_all[owner], ps_all[owner])
+    out_ref[...] = total.astype(BF16)
+
+    for copy in to_sib + to_oth + forward + gain_copies + [halo_up, halo_down] + first + second + cross + weight_copies + state_copies:
         copy.wait_send()
     repeat(1, n_sp, lambda r: interval_copy(r).wait_send())
     repeat(1, n_sp, lambda r: edge_copy(r).wait_send())
@@ -405,7 +428,10 @@
             pltpu.VMEM((dirs * 2 * groups, per), F32),
             pltpu.SMEM((1, rows), F32),
             pltpu.VMEM((width * n_tp, 4 * channels), BF16),
-            pltpu.VMEM((2 * channels, width * n_tp), BF16),
+            pltpu.VMEM((channels, width * n_tp), BF16),
+            pltpu.VMEM((n_tp, channels, width), BF16),
+            pltpu.VMEM((n_tp, rows, channels), BF16),
+            pltpu.VMEM((rows, width), F32),
             pltpu.VMEM((2, dirs * groups * group, per), F32),
             pltpu.VMEM((2, dirs * groups * group, per), F32),
             pltpu.VMEM((n_tp, CHUNKS, rows, cw), BF16),
@@ -425,11 +451,11 @@
             dma(CHUNKS), dma(CHUNKS), dma(CHUNKS), dma(CHUNKS), dma(CHUNKS), dma(CHUNKS),
             dma(n_tp), dma(n_tp), dma(n_sp), dma(n_sp), dma(2), dma(2), dma(n_sp), dma(n_sp),
             dma(OUT_CHUNKS), dma(OUT_CHUNKS), dma(OUT_CHUNKS), dma(OUT_CHUNKS),
-            dma(OUT_CHUNKS), dma(OUT_CHUNKS),
+            dma(OUT_CHUNKS), dma(OUT_CHUNKS), dma(n_tp), dma(n_tp), dma(n_tp), dma(n_tp),
         ],
         compiler_params=pltpu.CompilerParams(
-            collective_id=0, has_side_effects=True, vmem_limit_bytes=67043328),
-    )(
+            collective_id=0, has_side_effects=True, vmem_limit_bytes=48 * 1024 * 1024),
+    )(*(pltpu.with_memory_space_constraint(a, pltpu.HBM) for a in (
         stream, norm_gain.reshape(1, width), w_value, w_mix, w_gate, w_state, conv_taps,
         skip_gain.reshape(1, channels),
         decay_rate.reshape(dirs * groups, per), turn_rate.reshape(dirs * groups, per),
@@ -437,7 +463,7 @@
         read_real.reshape(dirs * groups * group, per), read_imag.reshape(dirs * groups * group, per),
         initial_state.reshape(dirs * 2 * groups, per), intervals.reshape(1, rows),
         proj_conv, proj_state,
-    )
+    )))
 
 
 def solution(mesh):

time: 26 us -> 25.4 us (0.977)
  local copies, waits for them, and re-layouts: 1.57 us -> 0.66 us
  Pallas kernels: 24.3 us -> 24.6 us
    unnamed x1, local copies, waits for them, and re-layouts: 1.57 us -> 0.66 us
where the time goes in v3:
time: 25.4 us; the launch traced here: 25.2 us
  Pallas kernels  24.6 us (97%)
  local copies, waits for them, and re-layouts  0.66 us (3%)
    pallas_call x1, Pallas kernels, per_device(): pl.pallas_call(functools.partial(kernel, n_sp, n_tp), out_shape=jax.Shape...  24.6 us
    unnamed x1, local copies, waits for them, and re-layouts  0.66 us

profile of v3, /device:TPU:0, one launch (start us, length us, event | category | flops | bytes accessed | tf_op | source)
XLA Modules:
  0.0 25.2 jit_solution(4269078722427927449)
XLA Ops:
  0.0 24.6 %shard_map.172 = bf16[128,512]{1,0:T(8,128)(2,1)S(1)} custom-call(bf16[128,512]{1,0:T(8,128)(2,1)} %x_hbm.1, f32[1,512]{1,0:T(1,128)} %bitcast.21, bf16[2048,128]{1,0:T(8,128)(2,1)} %wv.1, bf16[2048,128]{1,0:T(8,128)(2,1)} %wm.1, bf16[2048,128]{1,0:T(8,128)(2,1)} %wg.1, bf16[2048,128]{1,0:T(8,128)(2,1)} %ws.1, f32[3,128]{1,0:T(4,128)} %taps_hbm.1, ...), custom_call_target="tpu_custom_call" | custom-call | tf_op jit(solution)/shard_map/pallas_call | solution.py:416
  24.6 0.7 %copy.20 = bf16[128,512]{1,0:T(8,128)(2,1)} copy(bf16[128,512]{1,0:T(8,128)(2,1)S(1)} %shard_map.172) | data formatting | bytes 262144

commit v4 on v2

--- a/solution.py
+++ b/solution.py
@@ -428,8 +428,8 @@
             dma(OUT_CHUNKS), dma(OUT_CHUNKS),
         ],
         compiler_params=pltpu.CompilerParams(
-            collective_id=0, has_side_effects=True, vmem_limit_bytes=67043328),
-    )(
+            collective_id=0, has_side_effects=True, vmem_limit_bytes=48 * 1024 * 1024),
+    )(*(pltpu.with_memory_space_constraint(a, pltpu.HBM) for a in (
         stream, norm_gain.reshape(1, width), w_value, w_mix, w_gate, w_state, conv_taps,
         skip_gain.reshape(1, channels),
         decay_rate.reshape(dirs * groups, per), turn_rate.reshape(dirs * groups, per),
@@ -437,7 +437,7 @@
         read_real.reshape(dirs * groups * group, per), read_imag.reshape(dirs * groups * group, per),
         initial_state.reshape(dirs * 2 * groups, per), intervals.reshape(1, rows),
         proj_conv, proj_state,
-    )
+    )))
 
 
 def solution(mesh):

time: 26 us -> 24.5 us (0.942)
  local copies, waits for them, and re-layouts: 1.57 us -> 0.66 us
  Pallas kernels: 24.3 us -> 23.7 us
    unnamed x1, local copies, waits for them, and re-layouts: 1.57 us -> 0.66 us
    pallas_call x1, Pallas kernels: 24.3 us -> 23.7 us  [per_device(): pl.pallas_call(functools.partial(kernel, n_sp, n_tp), out_shape=jax.Shape...]
where the time goes in v4:
time: 24.5 us; the launch traced here: 24.3 us
  Pallas kernels  23.7 us (97%)
  local copies, waits for them, and re-layouts  0.66 us (3%)
    pallas_call x1, Pallas kernels, per_device(): pl.pallas_call(functools.partial(kernel, n_sp, n_tp), out_shape=jax.Shape...  23.7 us
    unnamed x1, local copies, waits for them, and re-layouts  0.66 us

profile of v4, /device:TPU:0, one launch (start us, length us, event | category | flops | bytes accessed | tf_op | source)
XLA Modules:
  0.0 24.3 jit_solution(9490704589748713097)
XLA Ops:
  0.0 23.7 %shard_map.172 = bf16[128,512]{1,0:T(8,128)(2,1)S(1)} custom-call(bf16[128,512]{1,0:T(8,128)(2,1)} %x_hbm.1, f32[1,512]{1,0:T(1,128)} %bitcast.21, bf16[2048,128]{1,0:T(8,128)(2,1)} %wv.1, bf16[2048,128]{1,0:T(8,128)(2,1)} %wm.1, bf16[2048,128]{1,0:T(8,128)(2,1)} %wg.1, bf16[2048,128]{1,0:T(8,128)(2,1)} %ws.1, f32[3,128]{1,0:T(4,128)} %taps_hbm.1, ...), custom_call_target="tpu_custom_call" | custom-call | tf_op jit(solution)/shard_map/pallas_call | solution.py:393
  23.7 0.7 %copy.20 = bf16[128,512]{1,0:T(8,128)(2,1)} copy(bf16[128,512]{1,0:T(8,128)(2,1)S(1)} %shard_map.172) | data formatting | bytes 262144
